TPU v7x, 32 devices: a whole 2x2x4 slice. The times are simulated.
32 devices in a mesh: ep: 4 (over z), tp: 8 (over y, x, core).
Axes of the slice: x: 2, y: 2, z: 4, core: 2. Of those that a mesh axis runs over, the one named last changes fastest.
Arguments:
- tokens: bfloat16 [640, 2048], P('ep', 'tp'), may hold values from -6 to 6
- cotangent: bfloat16 [640, 2048], P('ep', 'tp'), may hold values from -6 to 6
- routes: int32 [640, 2], P('ep'), may hold values from 0 to 23, all different within a row; in each aligned block of 160 rows (0 to 159, 160 to 319, ...) at most 14 rows name the same one
- gate_weights: float32 [640, 2], P('ep'), may hold values from 0.2 to 2.5
- expert_gate: bfloat16 [24, 2048, 512], P('ep', 'tp'), may hold values from -0.125 to 0.125
- expert_up: bfloat16 [24, 2048, 512], P('ep', 'tp'), may hold values from -0.125 to 0.125
- expert_down: bfloat16 [24, 512, 2048], P('ep', None, 'tp'), may hold values from -0.25 to 0.25
- shared_gate: bfloat16 [2048, 576], P('tp'), may hold values from -0.125 to 0.125
- shared_up: bfloat16 [2048, 576], P('tp'), may hold values from -0.125 to 0.125
- shared_down: bfloat16 [576, 2048], P(None, 'tp'), may hold values from -0.25 to 0.25
Outputs:
- token_grad: bfloat16 [640, 2048], P('ep', 'tp')
- weight_grad: float32 [640, 2], P('ep')
- expert_gate_grad: float32 [24, 2048, 512], P('ep', 'tp')
- expert_up_grad: float32 [24, 2048, 512], P('ep', 'tp')
- expert_down_grad: float32 [24, 512, 2048], P('ep', None, 'tp')
- shared_gate_grad: float32 [2048, 576], P('tp', 'ep')
- shared_up_grad: float32 [2048, 576], P('tp', 'ep')
- shared_down_grad: float32 [576, 2048], P('ep', 'tp')
- gate_rows_sq: float32 [24, 2048], P('ep', 'tp')
- up_rows_sq: float32 [24, 2048], P('ep', 'tp')
- down_rows_sq: float32 [24, 512], P('ep')
- shared_gate_rows_sq: float32 [2048], P('tp')
- shared_up_rows_sq: float32 [2048], P('tp')
- shared_down_rows_sq: float32 [576], P('ep')
Inputs may be any that keep to these rules, and one draw needn't show every extreme that they name: `routes`: each row names 2 different experts. Among the rows of one index of ep (aligned blocks of 160 rows) no expert is named more than 14 times, a bound that some block reaches.
All inputs are finite; a program needn't handle non-finite values.
Results may differ from a plain program's by a relative error of at most 0.0059.
Values may be sent and summed in bfloat16 or wider, within the bound.
A program may use at most 64 MiB of HBM per device.

v0:
```python
import jax
import jax.numpy as jnp
from jax import lax
from jax.sharding import PartitionSpec as P


def silu_parts(pre):
    logistic = jax.nn.sigmoid(pre)
    return (pre * logistic, logistic * (1.0 + pre * (1.0 - logistic)))


def activate(gate_sum, up_sum, back_sum, recv_w, s_gate, s_up, s_back):
    silu_out, silu_slope = silu_parts(gate_sum)
    hidden = (silu_out * up_sum).astype(jnp.bfloat16)
    dhidden = recv_w[:, :, None] * back_sum
    grad_gate = (dhidden * up_sum * silu_slope).astype(jnp.bfloat16)
    grad_up = (dhidden * silu_out).astype(jnp.bfloat16)
    dots = jnp.sum(hidden.astype(jnp.float32) * back_sum, axis=2)
    s_out, s_slope = silu_parts(s_gate)
    s_hidden = (s_out * s_up).astype(jnp.bfloat16)
    s_dgate = (s_back * s_up * s_slope).astype(jnp.bfloat16)
    s_dup = (s_back * s_out).astype(jnp.bfloat16)
    return (hidden, grad_gate, grad_up, dots, s_hidden, s_dgate, s_dup)


def per_device(
    tokens,
    cotangent,
    routes,
    gate_weights,
    expert_gate,
    expert_up,
    expert_down,
    shared_gate,
    shared_up,
    shared_down,
):
    tok_rows, narrow = tokens.shape
    picks_per = routes.shape[1]
    local_experts = expert_gate.shape[0]
    experts_all = local_experts * lax.axis_size("ep")
    capacity = max(2, (tok_rows * picks_per + experts_all - 1) // experts_all)
    owners = routes.reshape(-1)
    assigned = owners.shape[0]
    picked = (owners[:, None] == jnp.arange(experts_all, dtype=jnp.int32)[None, :]).astype(
        jnp.int32
    )
    slot_rank = jnp.sum((jnp.cumsum(picked, axis=0) - picked) * picked, axis=1)
    source_tok = jnp.arange(assigned, dtype=jnp.int32) // picks_per
    slot_tok = (
        jnp.full((capacity, experts_all), tok_rows, jnp.int32).at[slot_rank, owners].set(source_tok)
    )
    slot_weight = (
        jnp.zeros((capacity, experts_all), jnp.float32)
        .at[slot_rank, owners]
        .set(gate_weights.reshape(-1))
    )
    zero_row = jnp.zeros((1, narrow), tokens.dtype)
    sent_x = jnp.concatenate([tokens, zero_row], axis=0)[slot_tok]
    sent_dy = jnp.concatenate([cotangent, zero_row], axis=0)[slot_tok]
    recv_x, recv_dy = (
        lax.all_to_all(sent_x, "ep", split_axis=1, concat_axis=0, tiled=True),
        lax.all_to_all(sent_dy, "ep", split_axis=1, concat_axis=0, tiled=True),
    )
    recv_w = lax.all_to_all(slot_weight, "ep", split_axis=1, concat_axis=0, tiled=True)
    gate_part = jnp.einsum("rel,elf->ref", recv_x, expert_gate, preferred_element_type=jnp.float32)
    up_part = jnp.einsum("rel,elf->ref", recv_x, expert_up, preferred_element_type=jnp.float32)
    back_part = jnp.einsum("rel,efl->ref", recv_dy, expert_down, preferred_element_type=jnp.float32)
    s_gate_part = jnp.dot(tokens, shared_gate, preferred_element_type=jnp.float32)
    s_up_part = jnp.dot(tokens, shared_up, preferred_element_type=jnp.float32)
    s_back_part = jnp.einsum(
        "tl,sl->ts", cotangent, shared_down, preferred_element_type=jnp.float32
    )
    gate_sum, up_sum, back_sum, s_gate, s_up, s_back = lax.psum(
        (gate_part, up_part, back_part, s_gate_part, s_up_part, s_back_part), "tp"
    )
    hidden, grad_gate, grad_up, gate_grad, s_hidden, s_dgate, s_dup = activate(
        gate_sum, up_sum, back_sum, recv_w, s_gate, s_up, s_back
    )
    weighted = (recv_w[:, :, None] * recv_dy.astype(jnp.float32)).astype(jnp.bfloat16)
    down_grad = jnp.einsum("ref,rel->efl", hidden, weighted, preferred_element_type=jnp.float32)
    gate_wgrad = jnp.einsum("rel,ref->elf", recv_x, grad_gate, preferred_element_type=jnp.float32)
    up_wgrad = jnp.einsum("rel,ref->elf", recv_x, grad_up, preferred_element_type=jnp.float32)
    row_grad = (
        jnp.einsum("ref,elf->rel", grad_gate, expert_gate, preferred_element_type=jnp.float32)
        + jnp.einsum("ref,elf->rel", grad_up, expert_up, preferred_element_type=jnp.float32)
    ).astype(jnp.bfloat16)
    back_rows = lax.all_to_all(row_grad, "ep", split_axis=0, concat_axis=1, tiled=True)
    back_gate = lax.all_to_all(gate_grad, "ep", split_axis=0, concat_axis=1, tiled=True)
    flat_index = slot_rank * experts_all + owners
    routed = back_rows.reshape(capacity * experts_all, narrow)[flat_index].astype(jnp.float32)
    routed = routed.reshape(tok_rows, picks_per, narrow).sum(axis=1)
    weight_grad = back_gate.reshape(-1)[flat_index].reshape(tok_rows, picks_per)
    term_gate = jnp.einsum("tl,ts->ls", tokens, s_dgate, preferred_element_type=jnp.float32)
    term_up = jnp.einsum("tl,ts->ls", tokens, s_dup, preferred_element_type=jnp.float32)
    term_down = jnp.einsum("ts,tl->sl", s_hidden, cotangent, preferred_element_type=jnp.float32)
    shared_gate_grad, shared_up_grad, shared_down_grad = (
        lax.psum_scatter(term_gate, "ep", scatter_dimension=1, tiled=True),
        lax.psum_scatter(term_up, "ep", scatter_dimension=1, tiled=True),
        lax.psum_scatter(term_down, "ep", scatter_dimension=0, tiled=True),
    )
    shared_rows = jnp.einsum(
        "ts,ls->tl", s_dgate, shared_gate, preferred_element_type=jnp.float32
    ) + jnp.einsum("ts,ls->tl", s_dup, shared_up, preferred_element_type=jnp.float32)
    token_grad = (routed + shared_rows).astype(jnp.bfloat16)
    gate_rows_sq = jnp.sum(gate_wgrad * gate_wgrad, axis=2)
    up_rows_sq = jnp.sum(up_wgrad * up_wgrad, axis=2)
    down_rows_sq, shared_down_rows_sq = lax.psum(
        (
            jnp.sum(down_grad * down_grad, axis=2),
            jnp.sum(shared_down_grad * shared_down_grad, axis=1),
        ),
        "tp",
    )
    shared_gate_rows_sq, shared_up_rows_sq = lax.psum(
        (
            jnp.sum(shared_gate_grad * shared_gate_grad, axis=1),
            jnp.sum(shared_up_grad * shared_up_grad, axis=1),
        ),
        "ep",
    )
    return (
        token_grad,
        weight_grad,
        gate_wgrad,
        up_wgrad,
        down_grad,
        shared_gate_grad,
        shared_up_grad,
        shared_down_grad,
        gate_rows_sq,
        up_rows_sq,
        down_rows_sq,
        shared_gate_rows_sq,
        shared_up_rows_sq,
        shared_down_rows_sq,
    )


def solution(mesh):
    return jax.shard_map(
        per_device,
        mesh=mesh,
        in_specs=(
            P("ep", "tp"),
            P("ep", "tp"),
            P("ep", None),
            P("ep", None),
            P("ep", "tp", None),
            P("ep", "tp", None),
            P("ep", None, "tp"),
            P("tp", None),
            P("tp", None),
            P(None, "tp"),
        ),
        out_specs=(
            P("ep", "tp"),
            P("ep", None),
            P("ep", "tp", None),
            P("ep", "tp", None),
            P("ep", None, "tp"),
            P("tp", "ep"),
            P("tp", "ep"),
            P("ep", "tp"),
            P("ep", "tp"),
            P("ep", "tp"),
            P("ep", None),
            P("tp"),
            P("tp"),
            P("ep"),
        ),
        check_vma=False,
    )
```

profile of v0, /device:TPU:0, one launch (start us, length us, event | category | flops | bytes accessed | tf_op | source)
XLA Modules:
  0.0 251.2 jit_solution(17227434565805106463)
XLA Ops:
  7.2 0.9 copy.56
  8.1 0.1 eq.22
  8.2 0.1 reshape.138
  8.4 0.9 reduce-window.6
  9.3 0.2 slice_reduce_fusion
  9.7 17.0 %scatter_fusion.1 = s32[14,24]{1,0:T(8,128)S(1)} fusion(s32[14,24]{1,0:T(8,128)S(1)} %broadcast_in_dim.7, s32[320]{0:T(512)S(1)} %get-tuple-element.71, s32[320]{0:T(512)S(1)} %add_select_fusion), kind=kCustom, calls=%fused_computation.5 | custom fusion | bytes 6400 | tf_op jit(solution)/shard_map/scatter | solution.py:51
  26.9 2.0 gather_fusion.1
  29.0 0.7 copy.65
  29.7 6.4 %all-to-all-start.2 = ((bf16[14,24,256]{2,0,1:T(8,128)(2,1)}), bf16[14,24,256]{2,0,1:T(8,128)(2,1)S(1)}, u32[]{:S(2)}, u32[]{:S(2)}) async-start(bf16[14,24,256]{2,0,1:T(8,128)(2,1)} %copy.65), calls=%async_computation.2 | async-start | bytes 393216 | tf_op jit(solution)/shard_map/all_to_all | solution.py:62
  36.0 1.0 fusion.21
  37.0 1.0 fusion.20
  38.1 2.0 gather_fusion
  40.1 0.7 copy.63
  40.8 1.0 fusion.22
  41.9 1.7 all-to-all-done.2
  43.5 4.0 %all-to-all-start.1 = ((bf16[14,24,256]{2,0,1:T(8,128)(2,1)}), bf16[14,24,256]{2,0,1:T(8,128)(2,1)}, u32[]{:S(2)}, u32[]{:S(2)}) async-start(bf16[14,24,256]{2,0,1:T(8,128)(2,1)} %copy.63), calls=%async_computation.1 | async-start | bytes 393216 | tf_op jit(solution)/shard_map/all_to_all | solution.py:63
  47.6 1.7 copy.66
  49.3 1.0 all_to_all.71
  50.3 1.2 convolution_bitcast_fusion
  51.6 1.2 convolution_bitcast_fusion.1
  52.8 1.1 all-to-all-done.1
  53.8 1.6 copy.64
  55.5 1.7 all_to_all.67
  57.1 3.0 %convolution_bitcast_fusion.2 = f32[56,6,512]{2,0,1:T(8,128)} fusion(bf16[56,6,256]{2,0,1:T(8,128)(2,1)} %all_to_all.67, bf16[6,512,256]{2,1,0:T(8,128)(2,1)} %param.16), kind=kOutput, calls=%fused_computation.11 | convolution fusion | flops 88080384 | bytes 2433024 | tf_op jit(solution)/shard_map/rel,efl->ref/dot_general | solution.py:68
  60.2 72.4 %all-reduce.8.cloned.1.call-done = (f32[56,6,512]{2,0,1:T(8,128)}, f32[56,6,512]{2,0,1:T(8,128)}, f32[56,6,512]{2,0,1:T(8,128)}, f32[160,576]{1,0:T(8,128)}, f32[160,576]{1,0:T(8,128)}, /*index=5*/f32[160,576]{1,0:T(8,128)}) async-done(((f32[56,6,512]{2,0,1:T(8,128)}, f32[56,6,512]{2,0,1:T(8,128)}, f32[56,6,512]{2,0,1:T(8,128)}, f32[160,576]{1,0:T(8,128)}, f32[160,576]{1,0:T(8,128)}, ...) | async-done | bytes 3170320 | tf_op jit(solution)/shard_map/psum | solution.py:74
  132.6 2.2 fusion.6
  134.9 0.1 copy.60
  135.0 0.1 reshape.179
  135.2 17.0 %scatter_fusion = f32[14,24]{1,0:T(8,128)S(1)} fusion(f32[14,24]{1,0:T(8,128)S(1)} %broadcast_in_dim.6, s32[320]{0:T(512)S(1)} %get-tuple-element.71, f32[320]{0:T(512)S(1)} %reshape.179), kind=kCustom, calls=%fused_computation.4 | custom fusion | bytes 6400 | tf_op jit(solution)/shard_map/scatter | solution.py:56
  152.2 0.1 copy.61
  152.2 0.6 all_to_all.61
  152.9 4.6 %all-to-all-start = ((f32[14,4,6]{0,2,1:T(8,128)}), f32[14,4,6]{0,2,1:T(8,128)S(1)}, u32[]{:S(2)}, u32[]{:S(2)}) async-start(f32[14,4,6]{0,2,1:T(8,128)} %all_to_all.61), calls=%async_computation | async-start | bytes 32768 | tf_op jit(solution)/shard_map/all_to_all | solution.py:65
  157.5 5.6 %all-to-all-done = f32[14,4,6]{0,2,1:T(8,128)S(1)} async-done(((f32[14,4,6]{0,2,1:T(8,128)}), f32[14,4,6]{0,2,1:T(8,128)S(1)}, u32[]{:S(2)}, u32[]{:S(2)}) %all-to-all-start) | async-done | bytes 1376 | tf_op jit(solution)/shard_map/all_to_all | solution.py:65
  163.1 0.1 mul.95
  163.2 2.1 multiply_convert_fusion.4
  165.3 0.7 copy-done.4
  166.0 1.1 convolution_bitcast_fusion.3
  167.1 2.9 %multiply_reduce_fusion.3 = (f32[56,6]{0,1:T(8,128)S(1)}, bf16[56,6,512]{2,0,1:T(8,128)(2,1)}, bf16[56,6,512]{2,0,1:T(8,128)(2,1)}, bf16[56,6,512]{2,0,1:T(8,128)(2,1)}) fusion(f32[56,6,512]{2,0,1:T(8,128)} %get-tuple-element.76, f32[56,6,512]{2,0,1:T(8,128)} %get-tuple-element.75, f32[56,6,512]{2,0,1:T(8,128)} %get-tuple-element.74, f32[56,6]{0,1:T(8,128)S(1)} %mul.95), kind=kLoop, calls=%fused_computation.20 | loop fusion | flops 3268272 | bytes 3099264 | tf_op jit(solution)/shard_map/reduce_sum | solution.py:18
  170.1 0.6 copy.70
  170.7 3.3 %all-to-all-start.4 = ((f32[4,14,6]{1,2,0:T(8,128)}), f32[4,14,6]{1,2,0:T(8,128)S(1)}, u32[]{:S(2)}, u32[]{:S(2)}) async-start(f32[4,14,6]{1,2,0:T(8,128)} %copy.70), calls=%async_computation.4 | async-start | bytes 32768 | tf_op jit(solution)/shard_map/all_to_all | solution.py:89
  174.0 2.0 convolution_bitcast_fusion.4
  176.0 2.4 fusion.19
  178.4 2.9 %multiply_reduce_fusion.2 = (f32[6,256]{1,0:T(8,128)}, f32[6,256,512]{2,1,0:T(8,128)}) fusion(bf16[56,6,256]{2,0,1:T(8,128)(2,1)S(1)} %all_to_all.71, bf16[56,6,512]{2,0,1:T(8,128)(2,1)S(1)} %copy-done.2), kind=kOutput, calls=%fused_computation.8 | convolution fusion | flops 89651712 | bytes 3667968 | tf_op jit(solution)/shard_map/rel,ref->elf/dot_general | solution.py:82
  181.3 2.5 %multiply_reduce_fusion = (f32[6,512]{1,0:T(8,128)S(1)}, f32[6,512,256]{1,2,0:T(8,128)}) fusion(bf16[56,6,512]{2,0,1:T(8,128)(2,1)S(1)} %copy-done.8, bf16[56,6,256]{2,0,1:T(8,128)(2,1)S(1)} %copy-done.7, f32[56,6]{0,1:T(8,128)S(1)} %mul.95), kind=kOutput, calls=%fused_computation.6 | convolution fusion | flops 89908224 | bytes 3675456 | tf_op jit(solution)/shard_map/ref,rel->efl/dot_general | solution.py:81
  183.9 1.7 fusion.1
  185.5 0.7 copy.67
  186.3 5.0 %all-to-all-start.3 = ((bf16[56,6,256]{2,1,0:T(8,128)(2,1)}), bf16[56,6,256]{2,1,0:T(8,128)(2,1)S(1)}, u32[]{:S(2)}, u32[]{:S(2)}) async-start(bf16[56,6,256]{2,1,0:T(8,128)(2,1)} %copy.67), calls=%async_computation.3 | async-start | bytes 458752 | tf_op jit(solution)/shard_map/all_to_all | solution.py:88
  191.3 3.9 %multiply_reduce_fusion.1 = (f32[6,256]{1,0:T(8,128)}, f32[6,256,512]{2,1,0:T(8,128)}) fusion(bf16[56,6,256]{2,0,1:T(8,128)(2,1)S(1)} %all_to_all.71, bf16[56,6,512]{2,0,1:T(8,128)(2,1)} %get-tuple-element.85), kind=kOutput, calls=%fused_computation.7 | convolution fusion | flops 89651712 | bytes 3667968 | tf_op jit(solution)/shard_map/rel,ref->elf/dot_general | solution.py:83
  195.2 3.6 %copy.73 = f32[6,512,256]{2,1,0:T(8,128)} copy(f32[6,512,256]{1,2,0:T(8,128)} %get-tuple-element.93) | data formatting | bytes 6291456
  198.8 0.2 fusion.23
  199.0 0.1 copy.71
  199.1 0.1 reshape.141
  199.3 2.4 gather_fusion.3
  201.7 0.1 reshape.142
  201.9 0.7 copy.72
  202.6 2.0 gather_fusion.2
  204.6 0.2 reshape.144
  204.8 0.4 reduce_sum.85
  205.2 0.9 fusion.3
  206.1 1.0 multiply_reduce_fusion.4
  207.1 22.9 %all-reduce.3 = (f32[6,512]{1,0:T(8,128)}, f32[144]{0:T(256)}) all-reduce(f32[6,512]{1,0:T(8,128)S(1)} %get-tuple-element.92, f32[144]{0:T(256)S(1)} %multiply_reduce_fusion.4), channel_id=1, replica_groups=mesh['ep'=4,'tp'=8] {'tp'}, use_global_device_ids=true, to_apply=%region_19.20 | all-reduce | flops 3216 | bytes 25728 | tf_op jit(solution)/shard_map/psum | solution.py:108
  230.1 0.9 multiply_reduce_fusion.5
  231.0 0.9 multiply_reduce_fusion.6
  232.0 12.7 %all-reduce.5 = (f32[256]{0:T(256)}, f32[256]{0:T(256)}) all-reduce(f32[256]{0:T(256)S(1)} %multiply_reduce_fusion.6, f32[256]{0:T(256)S(1)} %multiply_reduce_fusion.5), channel_id=1, replica_groups=mesh['ep'=4,'tp'=8] {'ep'}, use_global_device_ids=true, to_apply=%region_21.22 | all-reduce | flops 512 | bytes 4096 | tf_op jit(solution)/shard_map/psum | solution.py:115
  (65 shorter events, 0.8 us)
Async XLA Ops:
  7.2 43.2 %copy-start = (bf16[6,256,512]{2,1,0:T(8,128)(2,1)S(1)}, bf16[6,256,512]{2,1,0:T(8,128)(2,1)}, u32[]{:S(2)}) copy-start(bf16[6,256,512]{2,1,0:T(8,128)(2,1)} %param.14) | copy-start | bytes 4718596
  9.7 17.1 %copy-start.3 = (bf16[160,256]{1,0:T(8,128)(2,1)S(1)}, bf16[160,256]{1,0:T(8,128)(2,1)}, u32[]{:S(2)}) copy-start(bf16[160,256]{1,0:T(8,128)(2,1)} %param.10) | copy-start | bytes 245764
  26.7 9.3 %copy-start.9 = (bf16[256,576]{0,1:T(8,128)(2,1)S(1)}, bf16[256,576]{0,1:T(8,128)(2,1)}, u32[]{:S(2)}) copy-start(bf16[256,576]{0,1:T(8,128)(2,1)} %param.18) | copy-start | bytes 884740
  26.9 10.1 %copy-start.14 = (bf16[160,256]{1,0:T(8,128)(2,1)S(1)}, bf16[160,256]{1,0:T(8,128)(2,1)}, u32[]{:S(2)}) copy-start(bf16[160,256]{1,0:T(8,128)(2,1)} %param.11) | copy-start | bytes 245764
  26.9 10.1 %copy-start.15 = (bf16[576,256]{1,0:T(8,128)(2,1)S(1)}, bf16[576,256]{1,0:T(8,128)(2,1)}, u32[]{:S(2)}) copy-start(bf16[576,256]{1,0:T(8,128)(2,1)} %param.19) | copy-start | bytes 884740
  29.7 13.9 %all-to-all-start.2 = ((bf16[14,24,256]{2,0,1:T(8,128)(2,1)}), bf16[14,24,256]{2,0,1:T(8,128)(2,1)S(1)}, u32[]{:S(2)}, u32[]{:S(2)}) async-start(bf16[14,24,256]{2,0,1:T(8,128)(2,1)} %copy.65), calls=%async_computation.2 | async-start | bytes 393216 | tf_op jit(solution)/shard_map/all_to_all | solution.py:62
  37.0 3.8 %copy-start.11 = (bf16[256,576]{0,1:T(8,128)(2,1)S(1)}, bf16[256,576]{0,1:T(8,128)(2,1)}, u32[]{:S(2)}) copy-start(bf16[256,576]{0,1:T(8,128)(2,1)} %param.17) | copy-start | bytes 884740
  43.5 4.1 %copy-start.13 = (bf16[14,24,256]{2,0,1:T(8,128)(2,1)}, bf16[14,24,256]{2,0,1:T(8,128)(2,1)S(1)}, u32[]{:S(2)}) copy-start(bf16[14,24,256]{2,0,1:T(8,128)(2,1)S(1)} %all-to-all-done.2) | copy-start | bytes 516100
  43.5 10.3 %all-to-all-start.1 = ((bf16[14,24,256]{2,0,1:T(8,128)(2,1)}), bf16[14,24,256]{2,0,1:T(8,128)(2,1)}, u32[]{:S(2)}, u32[]{:S(2)}) async-start(bf16[14,24,256]{2,0,1:T(8,128)(2,1)} %copy.63), calls=%async_computation.1 | async-start | bytes 393216 | tf_op jit(solution)/shard_map/all_to_all | solution.py:63
  47.5 85.1 %all-reduce.8.cloned.1.call-start = ((), (), s32[]{:S(2)}) async-start(), calls=%async_computation.11 | async-start | bytes 6586368 | tf_op jit(solution)/shard_map/psum | solution.py:74
  47.6 4.0 %copy-start.1 = (bf16[6,256,512]{2,1,0:T(8,128)(2,1)S(1)}, bf16[6,256,512]{2,1,0:T(8,128)(2,1)}, u32[]{:S(2)}) copy-start(bf16[6,256,512]{2,1,0:T(8,128)(2,1)} %param.15) | copy-start | bytes 4718596
  60.1 74.8 %copy-start.16 = (f32[160,2]{0,1:T(2,128)S(1)}, f32[160,2]{0,1:T(2,128)}, u32[]{:S(2)}) copy-start(f32[160,2]{0,1:T(2,128)} %param.13) | copy-start | bytes 3844
  60.1 146.0 %reduce-scatter.8.cloned.1.call-start = ((), (), s32[]{:S(2)}) async-start(), calls=%async_computation.10 | async-start | bytes 737280 | tf_op jit(solution)/shard_map/reduce_scatter | solution.py:100
  152.9 10.2 %all-to-all-start = ((f32[14,4,6]{0,2,1:T(8,128)}), f32[14,4,6]{0,2,1:T(8,128)S(1)}, u32[]{:S(2)}, u32[]{:S(2)}) async-start(f32[14,4,6]{0,2,1:T(8,128)} %all_to_all.61), calls=%async_computation | async-start | bytes 32768 | tf_op jit(solution)/shard_map/all_to_all | solution.py:65
  157.5 72.6 %reduce-scatter.6.cloned.1.call-start = ((), (), s32[]{:S(2)}) async-start(), calls=%async_computation.9 | async-start | bytes 737280 | tf_op jit(solution)/shard_map/reduce_scatter | solution.py:99
  165.3 0.7 copy-start.4
  170.7 15.6 %all-to-all-start.4 = ((f32[4,14,6]{1,2,0:T(8,128)}), f32[4,14,6]{1,2,0:T(8,128)S(1)}, u32[]{:S(2)}, u32[]{:S(2)}) async-start(f32[4,14,6]{1,2,0:T(8,128)} %copy.70), calls=%async_computation.4 | async-start | bytes 32768 | tf_op jit(solution)/shard_map/all_to_all | solution.py:89
  174.0 57.1 %reduce-scatter.4.cloned.1.call-start = ((), (), s32[]{:S(2)}) async-start(), calls=%async_computation.8 | async-start | bytes 737280 | tf_op jit(solution)/shard_map/reduce_scatter | solution.py:98
  176.0 2.4 copy-start.2
  178.4 2.9 %copy-start.7 = (bf16[56,6,256]{2,0,1:T(8,128)(2,1)S(1)}, bf16[56,6,256]{2,0,1:T(8,128)(2,1)}, u32[]{:S(2)}) copy-start(bf16[56,6,256]{2,0,1:T(8,128)(2,1)} %all_to_all.67) | copy-start | bytes 516100
  178.4 2.9 %copy-start.8 = (bf16[56,6,512]{2,0,1:T(8,128)(2,1)S(1)}, bf16[56,6,512]{2,0,1:T(8,128)(2,1)}, u32[]{:S(2)}) copy-start(bf16[56,6,512]{2,0,1:T(8,128)(2,1)} %get-tuple-element.83) | copy-start | bytes 1032196
  186.3 16.2 %all-to-all-start.3 = ((bf16[56,6,256]{2,1,0:T(8,128)(2,1)}), bf16[56,6,256]{2,1,0:T(8,128)(2,1)S(1)}, u32[]{:S(2)}, u32[]{:S(2)}) async-start(bf16[56,6,256]{2,1,0:T(8,128)(2,1)} %copy.67), calls=%async_computation.3 | async-start | bytes 458752 | tf_op jit(solution)/shard_map/all_to_all | solution.py:88
  195.2 3.6 %copy-start.6 = (bf16[160,576]{1,0:T(8,128)(2,1)S(1)}, bf16[160,576]{1,0:T(8,128)(2,1)}, u32[]{:S(2)}) copy-start(bf16[160,576]{1,0:T(8,128)(2,1)} %get-tuple-element.87) | copy-start | bytes 552964
  195.2 3.6 %copy-start.12 = (bf16[256,576]{0,1:T(8,128)(2,1)S(1)}, bf16[256,576]{0,1:T(8,128)(2,1)}, u32[]{:S(2)}) copy-start(bf16[256,576]{0,1:T(8,128)(2,1)} %param.17) | copy-start | bytes 884740
  202.5 2.7 %copy-start.5 = (bf16[160,576]{1,0:T(8,128)(2,1)S(1)}, bf16[160,576]{1,0:T(8,128)(2,1)}, u32[]{:S(2)}) copy-start(bf16[160,576]{1,0:T(8,128)(2,1)} %copy-done.4) | copy-start | bytes 552964
  202.5 2.7 %copy-start.10 = (bf16[256,576]{0,1:T(8,128)(2,1)S(1)}, bf16[256,576]{0,1:T(8,128)(2,1)}, u32[]{:S(2)}) copy-start(bf16[256,576]{0,1:T(8,128)(2,1)} %param.18) | copy-start | bytes 884740
Sparse Core Ops, SparseCore 0:
  60.2 72.3 all-reduce.7
  135.5 22.1 reduce-scatter.7
  167.2 19.7 reduce-scatter.5
  189.7 21.0 reduce-scatter.3
where the time goes:
time: 252 us; the launch traced here: 251 us
  waiting for transfers between devices  80.8 us (32%)
  local copies, waits for them, and re-layouts  59.6 us (24%)
  blocking collectives  35.7 us (14%)
  matrix products  28.3 us (11%)
  starting transfers between devices  23.3 us (9%)
  between operations  14.1 us (6%)
  other arithmetic  9.43 us (4%)
    psum x1, waiting for transfers between devices, per_device(): lax.psum((gate_part, up_part, back_part, s_gate_part, s_up_part, s_back_p...  72.4 us
    psum x1, blocking collectives, per_device(): lax.psum((jnp.sum(down_grad * down_grad, axis=2), jnp.sum(shared_down_gra...  22.9 us
    scatter x2, local copies, waits for them, and re-layouts, per_device(): slot_weight = jnp.zeros((capacity, experts_all), jnp.float32).at[slot_ran...  17.1 us
    scatter x1, local copies, waits for them, and re-layouts, per_device(): jnp.full((capacity, experts_all), tok_rows, jnp.int32).at[slot_rank, owners]  17 us
    psum x1, blocking collectives, per_device(): lax.psum((jnp.sum(shared_gate_grad * shared_gate_grad, axis=1), jnp.sum(s...  12.7 us
    all_to_all x1, starting transfers between devices, per_device(): lax.all_to_all(sent_x, 'ep', split_axis=1, concat_axis=0, tiled=True)  6.35 us
    unnamed x38, local copies, waits for them, and re-layouts  6.04 us
    all_to_all x1, waiting for transfers between devices, per_device(): lax.all_to_all(slot_weight, 'ep', split_axis=1, concat_axis=0, tiled=True)  5.6 us
  transfers between devices with their start and end apart: 9, of which 4 were waited for; matrix products, arithmetic and copies ran while one was open for 25% of the time, Pallas kernels for 0%

commit v1 on v0

--- a/solution.py
+++ b/solution.py
@@ -2,6 +2,13 @@
 import jax.numpy as jnp
 from jax import lax
 from jax.sharding import PartitionSpec as P
+from jax.lax import all_to_all, axis_size
+
+
+def produce_column(field):
+    low = all_to_all(jnp.stack(jnp.split(field, axis_size("ep"), axis=1), axis=0), "ep", 0, 0)
+    placed = jnp.concatenate(low, axis=0)
+    return placed
 
 
 def silu_parts(pre):
@@ -59,7 +66,7 @@
     sent_x = jnp.concatenate([tokens, zero_row], axis=0)[slot_tok]
     sent_dy = jnp.concatenate([cotangent, zero_row], axis=0)[slot_tok]
     recv_x, recv_dy = (
-        lax.all_to_all(sent_x, "ep", split_axis=1, concat_axis=0, tiled=True),
+        produce_column(sent_x),
         lax.all_to_all(sent_dy, "ep", split_axis=1, concat_axis=0, tiled=True),
     )
     recv_w = lax.all_to_all(slot_weight, "ep", split_axis=1, concat_axis=0, tiled=True)

time: 252 us -> 253 us (level)
  no operation moved by 1% of the time
where the time goes in v1:
time: 253 us; the launch traced here: 252 us
  waiting for transfers between devices  80.8 us (32%)
  local copies, waits for them, and re-layouts  59.6 us (24%)
  blocking collectives  35.7 us (14%)
  matrix products  28.3 us (11%)
  starting transfers between devices  23.3 us (9%)
  between operations  14.1 us (6%)
  other arithmetic  10.1 us (4%)
    psum x1, waiting for transfers between devices, per_device(): lax.psum((gate_part, up_part, back_part, s_gate_part, s_up_part, s_back_p...  72.4 us
    psum x1, blocking collectives, per_device(): lax.psum((jnp.sum(down_grad * down_grad, axis=2), jnp.sum(shared_down_gra...  22.9 us
    scatter x2, local copies, waits for them, and re-layouts, per_device(): slot_weight = jnp.zeros((capacity, experts_all), jnp.float32).at[slot_ran...  17.1 us
    scatter x1, local copies, waits for them, and re-layouts, per_device(): jnp.full((capacity, experts_all), tok_rows, jnp.int32).at[slot_rank, owners]  17 us
    psum x1, blocking collectives, per_device(): lax.psum((jnp.sum(shared_gate_grad * shared_gate_grad, axis=1), jnp.sum(s...  12.7 us
    unnamed x38, local copies, waits for them, and re-layouts  6.71 us
    all_to_all x1, starting transfers between devices, produce_column(): all_to_all(jnp.stack(jnp.split(field, axis_size('ep'), axis=1), axis=0),...  6.35 us
    all_to_all x1, waiting for transfers between devices, per_device(): lax.all_to_all(slot_weight, 'ep', split_axis=1, concat_axis=0, tiled=True)  5.6 us
  transfers between devices with their start and end apart: 9, of which 4 were waited for; matrix products, arithmetic and copies ran while one was open for 25% of the time, Pallas kernels for 0%

profile of v1, /device:TPU:0, one launch (start us, length us, event | category | flops | bytes accessed | tf_op | source)
XLA Modules:
  0.0 252.0 jit_solution(8376591710789150018)
XLA Ops:
  7.2 0.9 copy.64
  8.1 0.1 eq.22
  8.2 0.1 reshape.141
  8.4 0.9 reduce-window.6
  9.3 0.2 slice_reduce_fusion
  9.7 17.0 %scatter_fusion.1 = s32[14,24]{1,0:T(8,128)S(1)} fusion(s32[14,24]{1,0:T(8,128)S(1)} %broadcast_in_dim.7, s32[320]{0:T(512)S(1)} %get-tuple-element.71, s32[320]{0:T(512)S(1)} %add_select_fusion), kind=kCustom, calls=%fused_computation.5 | custom fusion | bytes 6400 | tf_op jit(solution)/shard_map/scatter | solution.py:58
  26.9 2.0 gather_fusion.1
  29.1 0.7 pad_maximum_fusion
  29.8 6.4 %all-to-all-start.2 = ((bf16[4,14,6,256]{3,1,2,0:T(8,128)(2,1)}), bf16[4,14,6,256]{3,1,2,0:T(8,128)(2,1)S(1)}, u32[]{:S(2)}, u32[]{:S(2)}) async-start(bf16[4,14,6,256]{3,1,2,0:T(8,128)(2,1)} %pad_maximum_fusion), calls=%async_computation.2 | async-start | bytes 393216 | tf_op jit(solution)/shard_map/all_to_all | solution.py:9
  36.1 1.0 fusion.22
  37.2 1.0 fusion.21
  38.2 2.0 gather_fusion
  40.2 0.7 copy.71
  40.9 1.0 fusion.23
  42.0 1.7 all-to-all-done.2
  43.6 0.7 copy-done.13
  44.3 4.0 %all-to-all-start.1 = ((bf16[14,24,256]{2,0,1:T(8,128)(2,1)}), bf16[14,24,256]{2,0,1:T(8,128)(2,1)}, u32[]{:S(2)}, u32[]{:S(2)}) async-start(bf16[14,24,256]{2,0,1:T(8,128)(2,1)} %copy.71), calls=%async_computation.1 | async-start | bytes 393216 | tf_op jit(solution)/shard_map/all_to_all | solution.py:70
  48.4 1.7 copy.77
  50.1 1.0 reshape.143
  51.1 1.2 convolution_bitcast_fusion
  52.3 1.2 convolution_bitcast_fusion.1
  53.6 1.1 all-to-all-done.1
  54.6 1.6 copy.72
  56.3 1.7 all_to_all.57
  57.9 3.0 %convolution_bitcast_fusion.2 = f32[56,6,512]{2,0,1:T(8,128)} fusion(bf16[56,6,256]{2,0,1:T(8,128)(2,1)} %all_to_all.57, bf16[6,512,256]{2,1,0:T(8,128)(2,1)} %param.16), kind=kOutput, calls=%fused_computation.11 | convolution fusion | flops 88080384 | bytes 2433024 | tf_op jit(solution)/shard_map/rel,efl->ref/dot_general | solution.py:75
  61.0 72.4 %all-reduce.8.cloned.1.call-done = (f32[56,6,512]{2,0,1:T(8,128)}, f32[56,6,512]{2,0,1:T(8,128)}, f32[56,6,512]{2,0,1:T(8,128)}, f32[160,576]{1,0:T(8,128)}, f32[160,576]{1,0:T(8,128)}, /*index=5*/f32[160,576]{1,0:T(8,128)}) async-done(((f32[56,6,512]{2,0,1:T(8,128)}, f32[56,6,512]{2,0,1:T(8,128)}, f32[56,6,512]{2,0,1:T(8,128)}, f32[160,576]{1,0:T(8,128)}, f32[160,576]{1,0:T(8,128)}, ...) | async-done | bytes 3170320 | tf_op jit(solution)/shard_map/psum | solution.py:81
  133.4 2.2 fusion.6
  135.7 0.1 copy.68
  135.8 0.1 reshape.183
  135.9 17.0 %scatter_fusion = f32[14,24]{1,0:T(8,128)S(1)} fusion(f32[14,24]{1,0:T(8,128)S(1)} %broadcast_in_dim.6, s32[320]{0:T(512)S(1)} %get-tuple-element.71, f32[320]{0:T(512)S(1)} %reshape.183), kind=kCustom, calls=%fused_computation.4 | custom fusion | bytes 6400 | tf_op jit(solution)/shard_map/scatter | solution.py:63
  152.9 0.1 copy.69
  153.0 0.6 all_to_all.51
  153.6 4.6 %all-to-all-start = ((f32[14,4,6]{0,2,1:T(8,128)}), f32[14,4,6]{0,2,1:T(8,128)S(1)}, u32[]{:S(2)}, u32[]{:S(2)}) async-start(f32[14,4,6]{0,2,1:T(8,128)} %all_to_all.51), calls=%async_computation | async-start | bytes 32768 | tf_op jit(solution)/shard_map/all_to_all | solution.py:72
  158.3 5.6 %all-to-all-done = f32[14,4,6]{0,2,1:T(8,128)S(1)} async-done(((f32[14,4,6]{0,2,1:T(8,128)}), f32[14,4,6]{0,2,1:T(8,128)S(1)}, u32[]{:S(2)}, u32[]{:S(2)}) %all-to-all-start) | async-done | bytes 1376 | tf_op jit(solution)/shard_map/all_to_all | solution.py:72
  163.9 2.1 multiply_convert_fusion.4
  166.1 0.7 copy-done.4
  166.8 1.1 convolution_bitcast_fusion.3
  167.9 2.9 %multiply_reduce_fusion.3 = (f32[56,6]{0,1:T(8,128)S(1)}, bf16[56,6,512]{2,0,1:T(8,128)(2,1)}, bf16[56,6,512]{2,0,1:T(8,128)(2,1)}, bf16[56,6,512]{2,0,1:T(8,128)(2,1)}) fusion(f32[56,6,512]{2,0,1:T(8,128)} %get-tuple-element.76, f32[56,6,512]{2,0,1:T(8,128)} %get-tuple-element.75, f32[56,6,512]{2,0,1:T(8,128)} %get-tuple-element.74, f32[56,6]{0,1:T(8,128)S(1)} %mul.95), kind=kLoop, calls=%fused_computation.20 | loop fusion | flops 3268272 | bytes 3099264 | tf_op jit(solution)/shard_map/reduce_sum | solution.py:25
  170.9 0.6 copy.81
  171.5 3.3 %all-to-all-start.4 = ((f32[4,14,6]{1,2,0:T(8,128)}), f32[4,14,6]{1,2,0:T(8,128)S(1)}, u32[]{:S(2)}, u32[]{:S(2)}) async-start(f32[4,14,6]{1,2,0:T(8,128)} %copy.81), calls=%async_computation.4 | async-start | bytes 32768 | tf_op jit(solution)/shard_map/all_to_all | solution.py:96
  174.8 2.0 convolution_bitcast_fusion.4
  176.8 2.4 fusion.20
  179.2 2.9 %multiply_reduce_fusion.2 = (f32[6,256]{1,0:T(8,128)}, f32[6,256,512]{2,1,0:T(8,128)}) fusion(bf16[56,6,256]{2,0,1:T(8,128)(2,1)S(1)} %reshape.143, bf16[56,6,512]{2,0,1:T(8,128)(2,1)S(1)} %copy-done.2), kind=kOutput, calls=%fused_computation.8 | convolution fusion | flops 89651712 | bytes 3667968 | tf_op jit(solution)/shard_map/rel,ref->elf/dot_general | solution.py:89
  182.1 2.5 %multiply_reduce_fusion = (f32[6,512]{1,0:T(8,128)S(1)}, f32[6,512,256]{1,2,0:T(8,128)}) fusion(bf16[56,6,512]{2,0,1:T(8,128)(2,1)S(1)} %copy-done.8, bf16[56,6,256]{2,0,1:T(8,128)(2,1)S(1)} %copy-done.7, f32[56,6]{0,1:T(8,128)S(1)} %mul.95), kind=kOutput, calls=%fused_computation.6 | convolution fusion | flops 89908224 | bytes 3675456 | tf_op jit(solution)/shard_map/ref,rel->efl/dot_general | solution.py:88
  184.6 1.7 fusion.1
  186.3 0.7 copy.78
  187.1 5.0 %all-to-all-start.3 = ((bf16[56,6,256]{2,1,0:T(8,128)(2,1)}), bf16[56,6,256]{2,1,0:T(8,128)(2,1)S(1)}, u32[]{:S(2)}, u32[]{:S(2)}) async-start(bf16[56,6,256]{2,1,0:T(8,128)(2,1)} %copy.78), calls=%async_computation.3 | async-start | bytes 458752 | tf_op jit(solution)/shard_map/all_to_all | solution.py:95
  192.1 3.9 %multiply_reduce_fusion.1 = (f32[6,256]{1,0:T(8,128)}, f32[6,256,512]{2,1,0:T(8,128)}) fusion(bf16[56,6,256]{2,0,1:T(8,128)(2,1)S(1)} %reshape.143, bf16[56,6,512]{2,0,1:T(8,128)(2,1)} %get-tuple-element.85), kind=kOutput, calls=%fused_computation.7 | convolution fusion | flops 89651712 | bytes 3667968 | tf_op jit(solution)/shard_map/rel,ref->elf/dot_general | solution.py:90
  195.9 3.6 %copy.84 = f32[6,512,256]{2,1,0:T(8,128)} copy(f32[6,512,256]{1,2,0:T(8,128)} %get-tuple-element.97) | data formatting | bytes 6291456
  199.6 0.2 fusion.24
  199.8 0.1 copy.82
  199.9 0.1 reshape.145
  200.0 2.4 gather_fusion.3
  202.5 0.1 reshape.146
  202.6 0.7 copy.83
  203.4 2.0 gather_fusion.2
  205.4 0.2 reshape.148
  205.6 0.4 reduce_sum.85
  206.0 0.9 fusion.3
  206.9 1.0 multiply_reduce_fusion.4
  207.9 22.9 %all-reduce.3 = (f32[6,512]{1,0:T(8,128)}, f32[144]{0:T(256)}) all-reduce(f32[6,512]{1,0:T(8,128)S(1)} %get-tuple-element.96, f32[144]{0:T(256)S(1)} %multiply_reduce_fusion.4), channel_id=1, replica_groups=mesh['ep'=4,'tp'=8] {'tp'}, use_global_device_ids=true, to_apply=%region_19.20 | all-reduce | flops 3216 | bytes 25728 | tf_op jit(solution)/shard_map/psum | solution.py:115
  230.8 0.9 multiply_reduce_fusion.5
  231.8 0.9 multiply_reduce_fusion.6
  232.8 12.7 %all-reduce.5 = (f32[256]{0:T(256)}, f32[256]{0:T(256)}) all-reduce(f32[256]{0:T(256)S(1)} %multiply_reduce_fusion.6, f32[256]{0:T(256)S(1)} %multiply_reduce_fusion.5), channel_id=1, replica_groups=mesh['ep'=4,'tp'=8] {'ep'}, use_global_device_ids=true, to_apply=%region_21.22 | all-reduce | flops 512 | bytes 4096 | tf_op jit(solution)/shard_map/psum | solution.py:122
  (68 shorter events, 0.9 us)
Async XLA Ops:
  7.2 43.9 %copy-start = (bf16[6,256,512]{2,1,0:T(8,128)(2,1)S(1)}, bf16[6,256,512]{2,1,0:T(8,128)(2,1)}, u32[]{:S(2)}) copy-start(bf16[6,256,512]{2,1,0:T(8,128)(2,1)} %param.14) | copy-start | bytes 4718596
  9.7 17.1 %copy-start.3 = (bf16[160,256]{1,0:T(8,128)(2,1)S(1)}, bf16[160,256]{1,0:T(8,128)(2,1)}, u32[]{:S(2)}) copy-start(bf16[160,256]{1,0:T(8,128)(2,1)} %param.10) | copy-start | bytes 245764
  26.9 9.2 %copy-start.9 = (bf16[256,576]{0,1:T(8,128)(2,1)S(1)}, bf16[256,576]{0,1:T(8,128)(2,1)}, u32[]{:S(2)}) copy-start(bf16[256,576]{0,1:T(8,128)(2,1)} %param.18) | copy-start | bytes 884740
  28.9 8.2 %copy-start.14 = (bf16[160,256]{1,0:T(8,128)(2,1)S(1)}, bf16[160,256]{1,0:T(8,128)(2,1)}, u32[]{:S(2)}) copy-start(bf16[160,256]{1,0:T(8,128)(2,1)} %param.11) | copy-start | bytes 245764
  28.9 8.2 %copy-start.15 = (bf16[576,256]{1,0:T(8,128)(2,1)S(1)}, bf16[576,256]{1,0:T(8,128)(2,1)}, u32[]{:S(2)}) copy-start(bf16[576,256]{1,0:T(8,128)(2,1)} %param.19) | copy-start | bytes 884740
  29.8 13.9 %all-to-all-start.2 = ((bf16[4,14,6,256]{3,1,2,0:T(8,128)(2,1)}), bf16[4,14,6,256]{3,1,2,0:T(8,128)(2,1)S(1)}, u32[]{:S(2)}, u32[]{:S(2)}) async-start(bf16[4,14,6,256]{3,1,2,0:T(8,128)(2,1)} %pad_maximum_fusion), calls=%async_computation.2 | async-start | bytes 393216 | tf_op jit(solution)/shard_map/all_to_all | solution.py:9
  37.2 3.8 %copy-start.11 = (bf16[256,576]{0,1:T(8,128)(2,1)S(1)}, bf16[256,576]{0,1:T(8,128)(2,1)}, u32[]{:S(2)}) copy-start(bf16[256,576]{0,1:T(8,128)(2,1)} %param.17) | copy-start | bytes 884740
  43.6 0.7 copy-start.13
  44.3 10.3 %all-to-all-start.1 = ((bf16[14,24,256]{2,0,1:T(8,128)(2,1)}), bf16[14,24,256]{2,0,1:T(8,128)(2,1)}, u32[]{:S(2)}, u32[]{:S(2)}) async-start(bf16[14,24,256]{2,0,1:T(8,128)(2,1)} %copy.71), calls=%async_computation.1 | async-start | bytes 393216 | tf_op jit(solution)/shard_map/all_to_all | solution.py:70
  48.3 4.0 %copy-start.1 = (bf16[6,256,512]{2,1,0:T(8,128)(2,1)S(1)}, bf16[6,256,512]{2,1,0:T(8,128)(2,1)}, u32[]{:S(2)}) copy-start(bf16[6,256,512]{2,1,0:T(8,128)(2,1)} %param.15) | copy-start | bytes 4718596
  48.3 85.1 %all-reduce.8.cloned.1.call-start = ((), (), s32[]{:S(2)}) async-start(), calls=%async_computation.11 | async-start | bytes 6586368 | tf_op jit(solution)/shard_map/psum | solution.py:81
  60.9 74.8 %copy-start.16 = (f32[160,2]{0,1:T(2,128)S(1)}, f32[160,2]{0,1:T(2,128)}, u32[]{:S(2)}) copy-start(f32[160,2]{0,1:T(2,128)} %param.13) | copy-start | bytes 3844
  60.9 146.0 %reduce-scatter.8.cloned.1.call-start = ((), (), s32[]{:S(2)}) async-start(), calls=%async_computation.10 | async-start | bytes 737280 | tf_op jit(solution)/shard_map/reduce_scatter | solution.py:107
  153.6 10.2 %all-to-all-start = ((f32[14,4,6]{0,2,1:T(8,128)}), f32[14,4,6]{0,2,1:T(8,128)S(1)}, u32[]{:S(2)}, u32[]{:S(2)}) async-start(f32[14,4,6]{0,2,1:T(8,128)} %all_to_all.51), calls=%async_computation | async-start | bytes 32768 | tf_op jit(solution)/shard_map/all_to_all | solution.py:72
  158.2 72.6 %reduce-scatter.6.cloned.1.call-start = ((), (), s32[]{:S(2)}) async-start(), calls=%async_computation.9 | async-start | bytes 737280 | tf_op jit(solution)/shard_map/reduce_scatter | solution.py:106
  166.1 0.7 copy-start.4
  171.5 15.6 %all-to-all-start.4 = ((f32[4,14,6]{1,2,0:T(8,128)}), f32[4,14,6]{1,2,0:T(8,128)S(1)}, u32[]{:S(2)}, u32[]{:S(2)}) async-start(f32[4,14,6]{1,2,0:T(8,128)} %copy.81), calls=%async_computation.4 | async-start | bytes 32768 | tf_op jit(solution)/shard_map/all_to_all | solution.py:96
  174.7 57.1 %reduce-scatter.4.cloned.1.call-start = ((), (), s32[]{:S(2)}) async-start(), calls=%async_computation.8 | async-start | bytes 737280 | tf_op jit(solution)/shard_map/reduce_scatter | solution.py:105
  176.8 2.4 copy-start.2
  179.2 2.9 %copy-start.7 = (bf16[56,6,256]{2,0,1:T(8,128)(2,1)S(1)}, bf16[56,6,256]{2,0,1:T(8,128)(2,1)}, u32[]{:S(2)}) copy-start(bf16[56,6,256]{2,0,1:T(8,128)(2,1)} %all_to_all.57) | copy-start | bytes 516100
  179.2 2.9 %copy-start.8 = (bf16[56,6,512]{2,0,1:T(8,128)(2,1)S(1)}, bf16[56,6,512]{2,0,1:T(8,128)(2,1)}, u32[]{:S(2)}) copy-start(bf16[56,6,512]{2,0,1:T(8,128)(2,1)} %get-tuple-element.83) | copy-start | bytes 1032196
  187.1 16.2 %all-to-all-start.3 = ((bf16[56,6,256]{2,1,0:T(8,128)(2,1)}), bf16[56,6,256]{2,1,0:T(8,128)(2,1)S(1)}, u32[]{:S(2)}, u32[]{:S(2)}) async-start(bf16[56,6,256]{2,1,0:T(8,128)(2,1)} %copy.78), calls=%async_computation.3 | async-start | bytes 458752 | tf_op jit(solution)/shard_map/all_to_all | solution.py:95
  195.9 3.6 %copy-start.6 = (bf16[160,576]{1,0:T(8,128)(2,1)S(1)}, bf16[160,576]{1,0:T(8,128)(2,1)}, u32[]{:S(2)}) copy-start(bf16[160,576]{1,0:T(8,128)(2,1)} %get-tuple-element.87) | copy-start | bytes 552964
  195.9 3.6 %copy-start.12 = (bf16[256,576]{0,1:T(8,128)(2,1)S(1)}, bf16[256,576]{0,1:T(8,128)(2,1)}, u32[]{:S(2)}) copy-start(bf16[256,576]{0,1:T(8,128)(2,1)} %param.17) | copy-start | bytes 884740
  203.3 2.7 %copy-start.5 = (bf16[160,576]{1,0:T(8,128)(2,1)S(1)}, bf16[160,576]{1,0:T(8,128)(2,1)}, u32[]{:S(2)}) copy-start(bf16[160,576]{1,0:T(8,128)(2,1)} %copy-done.4) | copy-start | bytes 552964
  203.3 2.7 %copy-start.10 = (bf16[256,576]{0,1:T(8,128)(2,1)S(1)}, bf16[256,576]{0,1:T(8,128)(2,1)}, u32[]{:S(2)}) copy-start(bf16[256,576]{0,1:T(8,128)(2,1)} %param.18) | copy-start | bytes 884740
Sparse Core Ops, SparseCore 0:
  61.0 72.3 all-reduce.7
  136.2 22.1 reduce-scatter.7
  168.0 19.6 reduce-scatter.5
  190.5 21.0 reduce-scatter.3
